TPU v7x, 32 devices: a whole 2x2x4 slice. The times are simulated.
32 devices in a mesh: kv: 16 (over z, y, x), tp: 2 (over core).
Axes of the slice: x: 2, y: 2, z: 4, core: 2. Of those that a mesh axis runs over, the one named last changes fastest.
Arguments:
- tokens: bfloat16 [256, 2048], P('kv', 'tp'), may hold values from -20 to 20
- attn_gain: bfloat16 [2048], replicated, may hold values from 0.099609375 to 1.8984375
- query_weight: bfloat16 [2048, 1024], P(None, 'tp'), may hold values from -0.125 to 0.125
- key_weight: bfloat16 [2048, 1024], P(None, 'tp'), may hold values from -0.125 to 0.125
- value_weight: bfloat16 [2048, 1024], P(None, 'tp'), may hold values from -0.125 to 0.125
- outgate_weight: bfloat16 [2048, 1024], P(None, 'tp'), may hold values from -0.125 to 0.125
- gate_weight: bfloat16 [2, 8, 2048], replicated, may hold values from -0.125 to 0.125
- forget_bias: float32 [8], replicated, may hold values from -1 to 4
- state_matrix: float32 [256, 8, 128, 128], P('kv', 'tp'), may hold values from -1.8 to 1.8
- state_norm: float32 [256, 8, 128], P('kv', 'tp'), may hold values from -1.8 to 1.8
- state_max: float32 [256, 8], P('kv', 'tp'), may hold values from -1 to 1
- out_weight: bfloat16 [1024, 2048], P(None, 'tp'), may hold values from -0.1875 to 0.1875
- mlp_gain: bfloat16 [2048], P('tp'), may hold values from 0.099609375 to 1.8984375
- up_weight: bfloat16 [2048, 8192], P('tp', 'kv'), may hold values from -0.125 to 0.125
- down_weight: bfloat16 [8192, 2048], P('kv', 'tp'), may hold values from -0.0625 to 0.0625
Outputs:
- result: bfloat16 [256, 2048], P('kv', 'tp')
- next_matrix: float32 [256, 8, 128, 128], P('kv', 'tp')
- next_norm: float32 [256, 8, 128], P('kv', 'tp')
- next_max: float32 [256, 8], P('kv', 'tp')
All inputs are finite; a program needn't handle non-finite values.
Results may differ from a plain program's by a relative error of at most 0.013.
Values may be sent and summed in bfloat16 or wider, within the bound.
A program may use at most 64 MiB of HBM per device.

v0:
```python
import jax
import jax.numpy as jnp
from jax import lax
from jax.sharding import PartitionSpec as P

epsilon = 1e-06


def body(
    tokens,
    attn_gain,
    query_weight,
    key_weight,
    value_weight,
    outgate_weight,
    gate_weight,
    forget_bias,
    state_matrix,
    state_norm,
    state_max,
    out_weight,
    mlp_gain,
    up_weight,
    down_weight,
):
    sequences = tokens.shape[0]
    local_heads = state_matrix.shape[1]
    head_dim = state_matrix.shape[2]
    width = query_weight.shape[1]
    model_width = attn_gain.shape[0]
    first_head = lax.axis_index("tp") * local_heads
    my_gates = lax.dynamic_slice_in_dim(gate_weight, first_head, local_heads, 1).reshape(
        2 * local_heads, model_width
    )
    my_bias = lax.dynamic_slice_in_dim(forget_bias, first_head, local_heads, 0)
    gain_full = attn_gain.astype(jnp.float32)
    seg_values = lax.all_gather(tokens, "tp", axis=1, tiled=True).astype(jnp.float32)
    scaled = (seg_values * gain_full).astype(jnp.bfloat16)

    def product(weight):
        return jnp.dot(scaled, weight, preferred_element_type=jnp.float32)

    gate_part = jnp.einsum("sd,gd->sg", scaled, my_gates, preferred_element_type=jnp.float32)
    squares = jnp.sum(seg_values * seg_values, axis=1)
    query_acc = product(query_weight)
    key_acc = product(key_weight)
    value_acc = product(value_weight)
    outgate_acc = product(outgate_weight)
    scale_in = lax.rsqrt(squares / model_width + epsilon)[:, None]
    query_rows = (query_acc * scale_in).reshape(sequences, local_heads, head_dim)
    key_rows = (key_acc * scale_in * head_dim ** (-0.5)).reshape(sequences, local_heads, head_dim)
    value_rows = (value_acc * scale_in).reshape(sequences, local_heads, head_dim)
    outgate = (outgate_acc * scale_in).reshape(sequences, local_heads, head_dim)
    gate_pre = gate_part * scale_in
    in_gate = gate_pre[:, :local_heads]
    forget_log = jax.nn.log_sigmoid(gate_pre[:, local_heads:] + my_bias)
    next_max = jnp.maximum(forget_log + state_max, in_gate)
    kept_share = jnp.exp(forget_log + state_max - next_max)
    admitted = jnp.exp(in_gate - next_max)
    next_matrix = (
        kept_share[:, :, None, None] * state_matrix
        + admitted[:, :, None, None] * key_rows[:, :, :, None] * value_rows[:, :, None, :]
    )
    next_norm = kept_share[:, :, None] * state_norm + admitted[:, :, None] * key_rows
    numerator = jnp.einsum(
        "shd,shde->she", query_rows, next_matrix, precision=lax.Precision.HIGHEST
    )
    denominator = jnp.sum(query_rows * next_norm, axis=2)
    head_out = numerator / jnp.maximum(jnp.abs(denominator), 1.0)[:, :, None]
    mixed = (head_out * jax.nn.sigmoid(outgate)).reshape(sequences, width).astype(jnp.bfloat16)
    attended = jnp.dot(
        lax.all_gather(mixed, "tp", axis=1, tiled=True),
        out_weight,
        preferred_element_type=jnp.float32,
    )
    residual = (tokens.astype(jnp.float32) + attended).astype(jnp.bfloat16)
    gain_mid = mlp_gain.astype(jnp.float32)
    rows_all = lax.all_gather(residual, "kv", axis=0, tiled=True)
    row_values = rows_all.astype(jnp.float32)
    row_squares = jnp.sum(row_values * row_values, axis=1)
    scaled_mid = (row_values * gain_mid).astype(jnp.bfloat16)
    partial_value = jnp.dot(scaled_mid, up_weight, preferred_element_type=jnp.float32)
    summed = lax.psum(partial_value.astype(jnp.bfloat16), "tp").astype(jnp.float32)
    total_squares = lax.psum(row_squares.astype(jnp.bfloat16), "tp").astype(jnp.float32)
    up_value = summed * lax.rsqrt(total_squares / model_width + epsilon)[:, None]
    hidden = jnp.square(jax.nn.relu(up_value)).astype(jnp.bfloat16)
    mixer_out = lax.psum_scatter(
        jnp.dot(hidden, down_weight, preferred_element_type=jnp.float32),
        "kv",
        scatter_dimension=0,
        tiled=True,
    )
    result = (residual.astype(jnp.float32) + mixer_out).astype(jnp.bfloat16)
    return (result, next_matrix, next_norm, next_max)


def solution(mesh):
    in_specs = (
        P("kv", "tp"),
        P(),
        P(None, "tp"),
        P(None, "tp"),
        P(None, "tp"),
        P(None, "tp"),
        P(),
        P(),
        P("kv", "tp", None, None),
        P("kv", "tp", None),
        P("kv", "tp"),
        P(None, "tp"),
        P("tp"),
        P("tp", "kv"),
        P("kv", "tp"),
    )
    out_specs = (P("kv", "tp"), P("kv", "tp", None, None), P("kv", "tp", None), P("kv", "tp"))
    return jax.shard_map(body, mesh=mesh, in_specs=in_specs, out_specs=out_specs, check_vma=False)
```

profile of v0, /device:TPU:0, one launch (start us, length us, event | category | flops | bytes accessed | tf_op | source)
XLA Modules:
  0.0 179.5 jit_solution(18217517377536054853)
XLA Ops:
  7.2 0.0 copy-start
  7.2 0.0 copy-start.7
  7.2 0.0 copy-start.10
  7.2 0.0 copy-start.5
  7.2 0.0 copy-start.8
  7.2 0.0 all-reduce.2.cloned.1.call-start
  7.3 0.8 convert_element_type.53
  8.1 2.2 %all_gather.9 = bf16[16,2048]{1,0:T(8,128)(2,1)S(1)} all-gather(bf16[16,1024]{1,0:T(8,128)(2,1)} %param.15), channel_id=1, replica_groups=mesh['kv'=16,'tp'=2] {'tp'}, dimensions={1}, use_global_device_ids=true | all-gather | bytes 98304 | tf_op jit(solution)/shard_map/all_gather | solution.py:37
  10.3 0.1 fusion.14
  10.4 0.0 copy-start.4
  10.4 1.9 %convolution_multiply_fusion.3 = f32[16,512]{1,0:T(8,128)S(1)} fusion(bf16[2048,512]{1,0:T(8,128)(2,1)} %param.17, bf16[16,2048]{1,0:T(8,128)(2,1)S(1)} %all_gather.9, f32[2048]{0:T(1024)S(1)} %convert_element_type.53, f32[16]{0:T(128)S(1)} %add_rsqrt_fusion.1), kind=kOutput, calls=%fused_computation.11 | convolution fusion | flops 33660928 | bytes 2203712 | tf_op jit(solution)/shard_map/dot_general | solution.py:41
  12.4 0.1 reshape.53
  12.5 0.0 copy-done.7
  12.5 0.0 copy-done.10
  12.5 0.1 dynamic_slice.7
  12.6 0.0 copy-done.5
  12.6 0.1 convolution_multiply_fusion.4
  12.8 0.0 copy-done.8
  12.8 0.1 subtract_exponential_fusion.1
  12.9 0.0 copy-start.6
  12.9 0.1 copy.19
  13.0 0.1 copy.20
  13.1 1.9 %fusion.3 = f32[16,512]{1,0:T(8,128)S(1)} fusion(bf16[2048,512]{1,0:T(8,128)(2,1)} %param.18, bf16[16,2048]{1,0:T(8,128)(2,1)S(1)} %all_gather.9, f32[2048]{0:T(1024)S(1)} %convert_element_type.53, f32[16]{0:T(128)S(1)} %add_rsqrt_fusion.1), kind=kOutput, calls=%fused_computation.12 | convolution fusion | flops 33669120 | bytes 2203712 | tf_op jit(solution)/shard_map/dot_general | solution.py:41
  15.0 0.1 broadcast_in_dim_reshape.4
  15.1 0.0 copy-done.4
  15.1 0.0 copy-start.2
  15.1 0.7 multiply_reduce_fusion
  15.8 1.9 %convolution_multiply_fusion.1 = f32[16,512]{1,0:T(8,128)S(1)} fusion(bf16[2048,512]{1,0:T(8,128)(2,1)} %param.19, bf16[16,2048]{1,0:T(8,128)(2,1)S(1)} %all_gather.9, f32[2048]{0:T(1024)S(1)} %convert_element_type.53, f32[16]{0:T(128)S(1)} %add_rsqrt_fusion.1), kind=kOutput, calls=%fused_computation.9 | convolution fusion | flops 33660928 | bytes 2203712 | tf_op jit(solution)/shard_map/dot_general | solution.py:41
  17.7 0.0 copy-done.6
  17.7 0.0 copy-done.2
  17.8 0.4 fusion.5
  18.2 3.0 %multiply_add_fusion = f32[16,4,128,128]{3,2,1,0:T(8,128)S(1)} fusion(f32[16,4,128,128]{3,2,1,0:T(8,128)} %param.23, f32[16,4,128]{2,1,0:T(4,128)S(1)} %mul.144, f32[16,4,128]{2,1,0:T(4,128)S(1)} %get-tuple-element.6, f32[16,4]{1,0:T(8,128)S(1)} %copy.19), kind=kLoop, calls=%fused_computation | loop fusion | flops 3145728 | bytes 8454400 | tf_op jit(solution)/shard_map/add | solution.py:61
  21.3 0.0 copy-start.1
  21.3 0.0 copy-start.3
  21.3 3.7 %fusion.24 = f32[16,4,1,128]{3,2,1,0:T(1,128)S(1)} fusion(f32[16,4,128,1]{2,3,1,0:T(1,128)S(1)} %bitcast.18, f32[16,4,128,128]{3,2,1,0:T(8,128)S(1)} %multiply_add_fusion), kind=kOutput, calls=%fused_computation.45 | convolution fusion | flops 12582912 | bytes 4259840 | tf_op jit(solution)/shard_map/shd,shde->she/dot_general | solution.py:65
  25.0 0.0 copy-done.1
  25.0 0.0 copy-start.9
  25.0 0.1 fusion.15
  25.1 2.0 %all_gather.10 = bf16[16,1024]{1,0:T(8,128)(2,1)S(1)} all-gather(bf16[16,512]{1,0:T(8,128)(2,1)S(1)} %bitcast.20), channel_id=1, replica_groups=mesh['kv'=16,'tp'=2] {'tp'}, dimensions={1}, use_global_device_ids=true | all-gather | bytes 49152 | tf_op jit(solution)/shard_map/all_gather | solution.py:72
  27.0 0.0 copy-done
  27.0 0.0 copy-done.3
  27.0 0.4 fusion
  27.4 45.4 %all_gather.11 = bf16[256,1024]{1,0:T(8,128)(2,1)S(1)} all-gather(bf16[16,1024]{1,0:T(8,128)(2,1)S(1)} %fusion), channel_id=1, replica_groups=mesh['kv'=16,'tp'=2] {'kv'}, dimensions={0}, use_global_device_ids=true | all-gather | bytes 557056 | tf_op jit(solution)/shard_map/all_gather | solution.py:78
  72.8 0.0 copy-done.9
  72.8 1.2 convolution_convert_fusion
  74.0 0.0 all-reduce.2.cloned.1.call-update
  74.0 0.0 reduce-scatter.2.cloned.1.call-start
  74.1 0.2 fusion.7
  74.2 2.5 %psum.15 = bf16[256]{0:T(256)(128)(2,1)S(1)} all-reduce(bf16[256]{0:T(256)(128)(2,1)S(1)} %fusion.7), channel_id=1, replica_groups=mesh['kv'=16,'tp'=2] {'tp'}, use_global_device_ids=true, to_apply=%region_4.5 | all-reduce | flops 256 | bytes 1024 | tf_op jit(solution)/shard_map/psum | solution.py:84
  76.7 11.5 %all-reduce.2.cloned.1.call-done = bf16[256,512]{1,0:T(8,128)(2,1)} async-done(((bf16[256,512]{1,0:T(8,128)(2,1)}), bf16[256,512]{1,0:T(8,128)(2,1)}) %all-reduce.2.cloned.1.call-update) | async-done | bytes 262160 | tf_op jit(solution)/shard_map/psum | solution.py:83
  88.3 2.8 %fusion.10 = f32[256,1024]{1,0:T(8,128)} fusion(bf16[512,1024]{1,0:T(8,128)(2,1)} %param.29, bf16[256,512]{1,0:T(8,128)(2,1)} %all-reduce.2.cloned.1.call-done, f32[256]{0:T(256)S(1)} %add_rsqrt_fusion), kind=kOutput, calls=%fused_computation.20 | convolution fusion | flops 269090816 | bytes 2360320 | tf_op jit(solution)/shard_map/dot_general | solution.py:88
  91.0 0.0 reduce-scatter.2.cloned.1.call-update
  91.1 80.1 %reduce-scatter.2.cloned.1.call-done = f32[16,1024]{1,0:T(8,128)} async-done(((f32[256,1024]{1,0:T(8,128)}), f32[16,1024]{1,0:T(8,128)}) %reduce-scatter.2.cloned.1.call-update) | async-done | bytes 65552 | tf_op jit(solution)/shard_map/reduce_scatter | solution.py:87
  171.2 1.5 add_convert_fusion
  (11 shorter events, 0.1 us)
Async XLA Ops:
  7.2 19.9 %copy-start = (bf16[1024,1024]{1,0:T(8,128)(2,1)S(1)}, bf16[1024,1024]{1,0:T(8,128)(2,1)}, u32[]{:S(2)}) copy-start(bf16[1024,1024]{1,0:T(8,128)(2,1)} %param.26) | copy-start | bytes 6291460
  7.2 5.3 %copy-start.7 = (bf16[1024]{0:T(1024)(128)(2,1)S(1)}, bf16[1024]{0:T(1024)(128)(2,1)}, u32[]{:S(2)}) copy-start(bf16[1024]{0:T(1024)(128)(2,1)} %param.27) | copy-start | bytes 6148
  7.2 5.3 %copy-start.10 = (f32[8]{0:T(128)S(1)}, f32[8]{0:T(128)}, u32[]{:S(2)}) copy-start(f32[8]{0:T(128)} %param.22) | copy-start | bytes 100
  7.2 5.4 %copy-start.5 = (bf16[2,8,2048]{2,1,0:T(8,128)(2,1)S(1)}, bf16[2,8,2048]{2,1,0:T(8,128)(2,1)}, u32[]{:S(2)}) copy-start(bf16[2,8,2048]{2,1,0:T(8,128)(2,1)} %param.21) | copy-start | bytes 196612
  7.2 5.6 %copy-start.8 = (f32[16,4]{0,1:T(4,128)S(1)}, f32[16,4]{0,1:T(4,128)}, u32[]{:S(2)}) copy-start(f32[16,4]{0,1:T(4,128)} %param.25) | copy-start | bytes 772
  7.2 81.0 %all-reduce.2.cloned.1.call-start = ((), (), s32[]{:S(2)}) async-start(), calls=%async_computation.1 | async-start | bytes 524288 | tf_op jit(solution)/shard_map/psum | solution.py:83
  10.4 4.6 %copy-start.4 = (f32[16,4,128]{2,1,0:T(4,128)S(1)}, f32[16,4,128]{2,1,0:T(4,128)}, u32[]{:S(2)}) copy-start(f32[16,4,128]{2,1,0:T(4,128)} %param.24) | copy-start | bytes 98308
  12.9 4.9 %copy-start.6 = (f32[16,4]{0,1:T(4,128)}, f32[16,4]{0,1:T(4,128)S(1)}, u32[]{:S(2)}) copy-start(f32[16,4]{0,1:T(4,128)S(1)} %get-tuple-element.8) | copy-start | bytes 772
  15.1 2.7 %copy-start.2 = (bf16[2048,512]{1,0:T(8,128)(2,1)S(1)}, bf16[2048,512]{1,0:T(8,128)(2,1)}, u32[]{:S(2)}) copy-start(bf16[2048,512]{1,0:T(8,128)(2,1)} %param.20) | copy-start | bytes 6291460
  21.3 3.7 %copy-start.1 = (f32[16,4,128,128]{3,2,1,0:T(8,128)}, f32[16,4,128,128]{3,2,1,0:T(8,128)S(1)}, u32[]{:S(2)}) copy-start(f32[16,4,128,128]{3,2,1,0:T(8,128)S(1)} %multiply_add_fusion) | copy-start | bytes 12582916
  21.3 5.8 %copy-start.3 = (bf16[16,1024]{1,0:T(8,128)(2,1)S(1)}, bf16[16,1024]{1,0:T(8,128)(2,1)}, u32[]{:S(2)}) copy-start(bf16[16,1024]{1,0:T(8,128)(2,1)} %param.15) | copy-start | bytes 98308
  25.0 47.9 %copy-start.9 = (bf16[1024,512]{1,0:T(8,128)(2,1)S(1)}, bf16[1024,512]{1,0:T(8,128)(2,1)}, u32[]{:S(2)}) copy-start(bf16[1024,512]{1,0:T(8,128)(2,1)} %param.28) | copy-start | bytes 3145732
  74.0 97.2 %reduce-scatter.2.cloned.1.call-start = ((), (), s32[]{:S(2)}) async-start(), calls=%async_computation.2 | async-start | bytes 1114112 | tf_op jit(solution)/shard_map/reduce_scatter | solution.py:87
Sparse Core Ops, SparseCore 0:
  74.1 14.0 all-reduce.1
  91.2 79.9 reduce-scatter.1
where the time goes:
time: 180 us; the launch traced here: 179 us
  waiting for transfers between devices  91.7 us (51%)
  blocking collectives  52 us (29%)
  matrix products  14.3 us (8%)
  between operations  14.3 us (8%)
  other arithmetic  6.56 us (4%)
    reduce_scatter x1, waiting for transfers between devices, body(): lax.psum_scatter(jnp.dot(hidden, down_weight, preferred_element_type=jnp....  80.1 us
    all_gather x1, blocking collectives, body(): rows_all = lax.all_gather(residual, 'kv', axis=0, tiled=True)  45.4 us
    psum x1, waiting for transfers between devices, body(): lax.psum(partial_value.astype(jnp.bfloat16), 'tp').astype(jnp.float32)  11.5 us
    dot_general x4, matrix products, product(): return jnp.dot(scaled, weight, preferred_element_type=jnp.float32)  6.2 us
    dot_general x1, matrix products, body(): jnp.einsum('shd,shde->she', query_rows, next_matrix, precision=lax.Precis...  3.66 us
  transfers between devices with their start and end apart: 2, of which 2 were waited for; matrix products, arithmetic and copies ran while one was open for 0% of the time, Pallas kernels for 0%

commit v1 on v0

--- a/solution.py
+++ b/solution.py
@@ -1,9 +1,291 @@
+import functools
+
 import jax
 import jax.numpy as jnp
 from jax import lax
+from jax.experimental import pallas as pl
+from jax.experimental.pallas import tpu as pltpu
 from jax.sharding import PartitionSpec as P
 
 epsilon = 1e-06
+MESH = pl.DeviceIdType.MESH
+
+
+def partner_of(index, step, count):
+    if count & (count - 1):
+        return lax.rem(index + step, count), lax.rem(index + count - step, count)
+    out = 0
+    bit = 1
+    while bit < count:
+        digit = lax.rem(lax.div(index, bit), 2)
+        out = out + bit * (1 - digit if step & bit else digit)
+        bit *= 2
+    return out, out
+
+
+def mixer_kernel(
+    layers,
+    plane,
+    cores,
+    model_width,
+    tokens_ref,
+    mixed_ref,
+    gain_ref,
+    out_hbm,
+    up_hbm,
+    down_hbm,
+    result_ref,
+    out_w,
+    up_w,
+    down_w,
+    mixed_all,
+    rows_all,
+    up_own,
+    part_send,
+    part_all,
+    down_own,
+    near_send,
+    near_all,
+    far_send,
+    far_all,
+    load_sem,
+    mixed_send_sem,
+    mixed_recv_sem,
+    row_send_sem,
+    row_recv_sem,
+    part_send_sem,
+    part_recv_sem,
+    near_send_sem,
+    near_recv_sem,
+    far_send_sem,
+    far_recv_sem,
+):
+    rows = tokens_ref.shape[0]
+    width = mixed_ref.shape[1]
+    hidden_width = up_w.shape[1]
+    me = lax.axis_index("kv")
+    core = lax.axis_index("tp")
+    layer = lax.div(me, plane)
+    spot = lax.rem(me, plane)
+    loads = [
+        pltpu.make_async_copy(src, dst, load_sem.at[i])
+        for i, (src, dst) in enumerate(((out_hbm, out_w), (up_hbm, up_w), (down_hbm, down_w)))
+    ]
+    for load in loads:
+        load.start()
+    layer_steps = [partner_of(layer, s, layers) for s in range(layers)]
+    spot_steps = [partner_of(spot, s, plane) for s in range(plane)]
+    core_steps = [partner_of(core, s, cores) for s in range(cores)]
+
+    def kv_id(at_layer, at_spot):
+        return {"kv": at_layer * plane + at_spot}
+
+    barrier = pltpu.get_barrier_semaphore()
+    for s in range(1, cores):
+        pl.semaphore_signal(barrier, inc=1, device_id={"tp": core_steps[s][0]}, device_id_type=MESH)
+    for s in range(1, plane):
+        pl.semaphore_signal(
+            barrier, inc=1, device_id=kv_id(layer, spot_steps[s][0]), device_id_type=MESH
+        )
+    for s in range(1, layers):
+        pl.semaphore_signal(
+            barrier, inc=1, device_id=kv_id(layer_steps[s][0], spot), device_id_type=MESH
+        )
+    pl.semaphore_wait(barrier, cores + plane + layers - 3)
+
+    started = []
+
+    def send(src, dst, send_sem, recv_sem, device):
+        copy = pltpu.make_async_remote_copy(
+            src_ref=src,
+            dst_ref=dst,
+            send_sem=send_sem,
+            recv_sem=recv_sem,
+            device_id=device,
+            device_id_type=MESH,
+        )
+        copy.start()
+        started.append(copy)
+
+    def arrived(ref, sem):
+        pltpu.make_async_copy(ref, ref, sem).wait()
+
+    for s in range(1, cores):
+        send(
+            mixed_ref,
+            mixed_all.at[s],
+            mixed_send_sem.at[s],
+            mixed_recv_sem.at[s],
+            {"tp": core_steps[s][0]},
+        )
+    loads[0].wait()
+
+    def out_part(values, owner):
+        block = out_w[pl.ds(pl.multiple_of(owner * width, width), width), :]
+        return jnp.dot(values, block, preferred_element_type=jnp.float32)
+
+    attended = out_part(mixed_ref[...], core)
+    for s in range(1, cores):
+        arrived(mixed_all.at[s], mixed_recv_sem.at[s])
+        attended = attended + out_part(mixed_all[s], core_steps[s][1])
+    residual = (tokens_ref[...].astype(jnp.float32) + attended).astype(jnp.bfloat16)
+    rows_all[0, 0] = residual
+    for s in range(1, layers):
+        send(
+            rows_all.at[0, 0],
+            rows_all.at[s, 0],
+            row_send_sem.at[s, 0],
+            row_recv_sem.at[s, 0],
+            kv_id(layer_steps[s][0], spot),
+        )
+
+    def spread(g):
+        for s in range(1, plane):
+            send(
+                rows_all.at[g, 0],
+                rows_all.at[g, s],
+                row_send_sem.at[g, s],
+                row_recv_sem.at[g, s],
+                kv_id(layer, spot_steps[s][0]),
+            )
+
+    spread(0)
+    gain = gain_ref[...].astype(jnp.float32)
+    group = plane * rows
+
+    def up_stage(g):
+        if g + 1 < layers:
+            arrived(rows_all.at[g + 1, 0], row_recv_sem.at[g + 1, 0])
+            spread(g + 1)
+        for s in range(1, plane):
+            arrived(rows_all.at[g, s], row_recv_sem.at[g, s])
+        if g == 0:
+            loads[1].wait()
+        values = rows_all[g].reshape(group, -1).astype(jnp.float32)
+        squares = jnp.sum(values * values, axis=1, keepdims=True)
+        high = squares.astype(jnp.bfloat16).astype(jnp.float32)
+        lanes = lax.broadcasted_iota(jnp.int32, (group, 128), 1)
+        part_send[g, :, hidden_width:] = jnp.where(lanes < 64, high, squares - high).astype(jnp.bfloat16)
+        scaled = (values * gain).astype(jnp.bfloat16)
+        partial = jnp.dot(scaled, up_w[...], preferred_element_type=jnp.float32)
+        part_send[g, :, :hidden_width] = partial.astype(jnp.bfloat16)
+        for s in range(1, cores):
+            send(
+                part_send.at[g],
+                part_all.at[g, s],
+                part_send_sem.at[g, s],
+                part_recv_sem.at[g, s],
+                {"tp": core_steps[s][0]},
+            )
+        up_own[g, :, :hidden_width] = partial
+        up_own[g, :, hidden_width:] = jnp.broadcast_to(squares, (group, 128))
+
+    def down_stage(g):
+        total = up_own[g, :, :hidden_width]
+        squares = up_own[g, :, hidden_width : hidden_width + 1]
+        for s in range(1, cores):
+            arrived(part_all.at[g, s], part_recv_sem.at[g, s])
+            total = total + part_all[g, s, :, :hidden_width].astype(jnp.float32)
+            tail = part_all[g, s, :, hidden_width:].astype(jnp.float32)
+            squares = squares + tail[:, 0:1] + tail[:, 64:65]
+        up_value = total * lax.rsqrt(squares / model_width + epsilon)
+        hidden = jnp.square(jnp.maximum(up_value, 0.0)).astype(jnp.bfloat16)
+        if g == 0:
+            loads[2].wait()
+        share = jnp.dot(hidden, down_w[...], preferred_element_type=jnp.float32)
+        down_own[g] = share[:rows]
+        near_send[g] = share.astype(jnp.bfloat16).reshape(near_send.shape[1:])
+        for s in range(1, plane):
+            send(
+                near_send.at[g, s],
+                near_all.at[g, s],
+                near_send_sem.at[g, s],
+                near_recv_sem.at[g, s],
+                kv_id(layer, spot_steps[s][1]),
+            )
+
+    def plane_sum(g):
+        total = down_own[g]
+        for s in range(1, plane):
+            arrived(near_all.at[g, s], near_recv_sem.at[g, s])
+            total = total + near_all[g, s].astype(jnp.float32)
+        return total
+
+    def far_stage(g):
+        total = plane_sum(g)
+        if g == 0:
+            down_own[0] = total
+            return
+        far_send[g] = total.astype(jnp.bfloat16)
+        send(
+            far_send.at[g],
+            far_all.at[g],
+            far_send_sem.at[g],
+            far_recv_sem.at[g],
+            kv_id(layer_steps[g][1], spot),
+        )
+
+    for g in range(layers + 2):
+        if g < layers:
+            up_stage(g)
+        if 0 <= g - 1 < layers:
+            down_stage(g - 1)
+        if 0 <= g - 2 < layers:
+            far_stage(g - 2)
+    total = down_own[0]
+    for s in range(1, layers):
+        arrived(far_all.at[s], far_recv_sem.at[s])
+        total = total + far_all[s].astype(jnp.float32)
+    result_ref[...] = (rows_all[0, 0].astype(jnp.float32) + total).astype(jnp.bfloat16)
+    for copy in started:
+        copy.wait_send()
+
+
+def channel_mixer(tokens, mixed, mlp_gain, out_weight, up_weight, down_weight, model_width):
+    count = lax.axis_size("kv")
+    cores = lax.axis_size("tp")
+    plane = 4 if count % 4 == 0 else 1
+    layers = count // plane
+    rows, features = tokens.shape
+    hidden_width = up_weight.shape[1]
+    group = plane * rows
+    bf16, f32, dma = jnp.bfloat16, jnp.float32, pltpu.SemaphoreType.DMA
+    vmem = pl.BlockSpec(memory_space=pltpu.VMEM)
+    anywhere = pl.BlockSpec(memory_space=pl.ANY)
+    return pl.pallas_call(
+        functools.partial(mixer_kernel, layers, plane, cores, model_width),
+        out_shape=jax.ShapeDtypeStruct((rows, features), bf16),
+        in_specs=[vmem] * 3 + [anywhere] * 3,
+        out_specs=vmem,
+        scratch_shapes=[
+            pltpu.VMEM(out_weight.shape, bf16),
+            pltpu.VMEM(up_weight.shape, bf16),
+            pltpu.VMEM(down_weight.shape, bf16),
+            pltpu.VMEM((cores,) + mixed.shape, bf16),
+            pltpu.VMEM((layers, plane, rows, features), bf16),
+            pltpu.VMEM((layers, group, hidden_width + 128), f32),
+            pltpu.VMEM((layers, group, hidden_width + 128), bf16),
+            pltpu.VMEM((layers, cores, group, hidden_width + 128), bf16),
+            pltpu.VMEM((layers, rows, features), f32),
+            pltpu.VMEM((layers, plane, rows, features), bf16),
+            pltpu.VMEM((layers, plane, rows, features), bf16),
+            pltpu.VMEM((layers, rows, features), bf16),
+            pltpu.VMEM((layers, rows, features), bf16),
+            dma((3,)),
+            dma((cores,)),
+            dma((cores,)),
+            dma((layers, plane)),
+            dma((layers, plane)),
+            dma((layers, cores)),
+            dma((layers, cores)),
+            dma((layers, plane)),
+            dma((layers, plane)),
+            dma((layers,)),
+            dma((layers,)),
+        ],
+        compiler_params=pltpu.CompilerParams(collective_id=0, has_side_effects=True),
+        name="channel_mixer",
+    )(tokens, mixed, mlp_gain.reshape(1, features), out_weight, up_weight, down_weight)
 
 
 def body(
@@ -68,29 +350,9 @@
     denominator = jnp.sum(query_rows * next_norm, axis=2)
     head_out = numerator / jnp.maximum(jnp.abs(denominator), 1.0)[:, :, None]
     mixed = (head_out * jax.nn.sigmoid(outgate)).reshape(sequences, width).astype(jnp.bfloat16)
-    attended = jnp.dot(
-        lax.all_gather(mixed, "tp", axis=1, tiled=True),
-        out_weight,
-        preferred_element_type=jnp.float32,
-    )
-    residual = (tokens.astype(jnp.float32) + attended).astype(jnp.bfloat16)
-    gain_mid = mlp_gain.astype(jnp.float32)
-    rows_all = lax.all_gather(residual, "kv", axis=0, tiled=True)
-    row_values = rows_all.astype(jnp.float32)
-    row_squares = jnp.sum(row_values * row_values, axis=1)
-    scaled_mid = (row_values * gain_mid).astype(jnp.bfloat16)
-    partial_value = jnp.dot(scaled_mid, up_weight, preferred_element_type=jnp.float32)
-    summed = lax.psum(partial_value.astype(jnp.bfloat16), "tp").astype(jnp.float32)
-    total_squares = lax.psum(row_squares.astype(jnp.bfloat16), "tp").astype(jnp.float32)
-    up_value = summed * lax.rsqrt(total_squares / model_width + epsilon)[:, None]
-    hidden = jnp.square(jax.nn.relu(up_value)).astype(jnp.bfloat16)
-    mixer_out = lax.psum_scatter(
-        jnp.dot(hidden, down_weight, preferred_element_type=jnp.float32),
-        "kv",
-        scatter_dimension=0,
-        tiled=True,
-    )
-    result = (residual.astype(jnp.float32) + mixer_out).astype(jnp.bfloat16)
+    result = channel_mixer(
+        tokens, mixed, mlp_gain, out_weight, up_weight, down_weight, model_width
+    )
     return (result, next_matrix, next_norm, next_max)
 
 

time: 180 us -> 52.3 us (0.29)
  waiting for transfers between devices: 91.7 us -> 0 us
  blocking collectives: 52 us -> 2.34 us
  Pallas kernels: 0 us -> 30.8 us
  between operations: 14.3 us -> 0.82 us
  matrix products: 14.3 us -> 10 us
  local copies, waits for them, and re-layouts: 0.52 us -> 3.14 us
    reduce_scatter x1 -> x0, waiting for transfers between devices: 80.1 us -> none  [body(): lax.psum_scatter(jnp.dot(hidden, down_weight, preferred_element_type=jnp....]
    all_gather x2 -> x0, blocking collectives: 47.4 us -> none  [the longest x1 45.4 us: body(): rows_all = lax.all_gather(residual, 'kv', axis=0, tiled=True)]
    pallas_call x0 -> x1, Pallas kernels: none -> 30.8 us  [channel_mixer(): pl.pallas_call(functools.partial(mixer_kernel, layers, plane, cores, mode...]
    psum x1 -> x0, waiting for transfers between devices: 11.5 us -> none  [body(): lax.psum(partial_value.astype(jnp.bfloat16), 'tp').astype(jnp.float32)]
    dot_general x3 -> x0, matrix products: 4.33 us -> none  [the longest x1 2.79 us: body(): jnp.dot(hidden, down_weight, preferred_element_type=jnp.float32)]
    psum x1 -> x0, blocking collectives: 2.47 us -> none  [body(): lax.psum(row_squares.astype(jnp.bfloat16), 'tp').astype(jnp.float32)]
    unnamed x23 -> x18, local copies, waits for them, and re-layouts: 0.07 us -> 2.04 us
  transfers between devices with their start and end apart: 2 -> 0, of which waited for: 2 -> 0; matrix products, arithmetic and copies ran while one was open for 0% -> 0% of each run, Pallas kernels for 0% -> 0%
where the time goes in v1:
time: 52.3 us; the launch traced here: 51.9 us
  Pallas kernels  30.8 us (59%)
  matrix products  10 us (19%)
  other arithmetic  4.78 us (9%)
  local copies, waits for them, and re-layouts  3.14 us (6%)
  blocking collectives  2.34 us (4%)
  between operations  0.82 us (2%)
    pallas_call x1, Pallas kernels, channel_mixer(): pl.pallas_call(functools.partial(mixer_kernel, layers, plane, cores, mode...  30.8 us
    dot_general x4, matrix products, product(): return jnp.dot(scaled, weight, preferred_element_type=jnp.float32)  6.22 us
    dot_general x1, matrix products, body(): jnp.einsum('shd,shde->she', query_rows, next_matrix, precision=lax.Precis...  3.66 us
    add x1, other arithmetic, body(): kept_share[:, :, None, None] * state_matrix  3.04 us
    all_gather x1, blocking collectives, body(): lax.all_gather(tokens, 'tp', axis=1, tiled=True).astype(jnp.float32)  2.34 us
    unnamed x18, local copies, waits for them, and re-layouts  2.04 us

profile of v1, /device:TPU:0, one launch (start us, length us, event | category | flops | bytes accessed | tf_op | source)
XLA Modules:
  0.0 51.9 jit_solution(7572036342176069293)
XLA Ops:
  0.6 0.0 copy-start
  0.6 2.3 %all_gather.3 = bf16[16,2048]{1,0:T(8,128)(2,1)S(1)} all-gather(bf16[16,1024]{1,0:T(8,128)(2,1)} %tokens_ref.1), channel_id=1, replica_groups=mesh['kv'=16,'tp'=2] {'tp'}, dimensions={1}, use_global_device_ids=true | all-gather | bytes 98304 | tf_op jit(solution)/shard_map/all_gather | solution.py:319
  3.0 0.7 %convert_element_type.15 = f32[2048]{0:T(1024)S(1)} convert(bf16[2048]{0:T(1024)(128)(2,1)} %param.16) | non-fusion elementwise | flops 2048 | bytes 12288 | tf_op jit(solution)/shard_map/convert_element_type | solution.py:318
  3.7 0.1 fusion.6
  3.8 0.0 copy-done
  3.8 0.4 fusion.4
  4.2 0.0 copy-start.3
  4.3 0.0 copy-start.7
  4.3 0.0 copy-start.6
  4.3 2.0 %convolution_multiply_fusion.3 = f32[16,512]{1,0:T(8,128)S(1)} fusion(bf16[2048,512]{1,0:T(8,128)(2,1)} %param.17, bf16[16,2048]{1,0:T(8,128)(2,1)S(1)} %all_gather.3, f32[2048]{0:T(1024)S(1)} %convert_element_type.15, f32[16]{0:T(128)S(1)} %add_rsqrt_fusion), kind=kOutput, calls=%fused_computation.6 | convolution fusion | flops 33660928 | bytes 2203712 | tf_op jit(solution)/shard_map/dot_general | solution.py:323
  6.2 0.1 reshape.55
  6.3 0.0 copy-start.2
  6.3 1.9 %convolution_multiply_fusion.1 = f32[16,512]{1,0:T(8,128)S(1)} fusion(bf16[2048,512]{1,0:T(8,128)(2,1)} %param.19, bf16[16,2048]{1,0:T(8,128)(2,1)S(1)} %all_gather.3, f32[2048]{0:T(1024)S(1)} %convert_element_type.15, f32[16]{0:T(128)S(1)} %add_rsqrt_fusion), kind=kOutput, calls=%fused_computation.4 | convolution fusion | flops 33660928 | bytes 2203712 | tf_op jit(solution)/shard_map/dot_general | solution.py:323
  8.3 0.1 mul.125
  8.3 0.0 copy-done.3
  8.4 0.1 convolution_multiply_fusion.4
  8.5 0.0 copy-done.7
  8.6 0.1 dynamic_slice.7
  8.6 0.0 copy-done.6
  8.6 0.1 subtract_exponential_fusion.1
  8.7 0.0 copy-start.4
  8.7 0.1 copy.19
  8.8 1.9 %fusion.2 = f32[16,512]{1,0:T(8,128)S(1)} fusion(bf16[2048,512]{1,0:T(8,128)(2,1)} %param.18, bf16[16,2048]{1,0:T(8,128)(2,1)S(1)} %all_gather.3, f32[2048]{0:T(1024)S(1)} %convert_element_type.15, f32[16]{0:T(128)S(1)} %add_rsqrt_fusion), kind=kOutput, calls=%fused_computation.7 | convolution fusion | flops 33669120 | bytes 2203712 | tf_op jit(solution)/shard_map/dot_general | solution.py:323
  10.8 0.1 broadcast_in_dim_reshape.4
  10.8 0.1 copy.20
  10.9 0.0 copy-done.2
  10.9 0.7 %multiply_reduce_fusion = (f32[16,4]{1,0:T(8,128)S(1)}, f32[16,4,128]{2,1,0:T(4,128)}, f32[16,4,128]{2,1,0:T(4,128)S(1)}) fusion(f32[16,4,128]{2,1,0:T(4,128)S(1)} %reshape.52, f32[16,4,128]{2,1,0:T(4,128)S(1)} %copy-done.2, f32[16,4]{1,0:T(8,128)S(1)} %copy.19, f32[16,4,128]{2,1,0:T(4,128)S(1)} %broadcast_in_dim_reshape.4, f32[16,4]{1,0:T(8,128)S(1)} %copy.20), kind=kLoop, calls=%fused_computation.16 | loop fusion | flops 40896 | bytes 164608 | tf_op jit(solution)/shard_map/reduce_sum | solution.py:350
  11.6 3.0 %multiply_add_fusion = f32[16,4,128,128]{3,2,1,0:T(8,128)S(1)} fusion(f32[16,4,128,128]{3,2,1,0:T(8,128)} %param.23, f32[16,4,128]{2,1,0:T(4,128)S(1)} %mul.125, f32[16,4,128]{2,1,0:T(4,128)S(1)} %get-tuple-element.6, f32[16,4]{1,0:T(8,128)S(1)} %copy.19), kind=kLoop, calls=%fused_computation | loop fusion | flops 3145728 | bytes 8454400 | tf_op jit(solution)/shard_map/add | solution.py:343
  14.7 0.0 copy-done.4
  14.7 0.0 copy-start.1
  14.7 0.0 copy-start.5
  14.7 3.7 %fusion.15 = f32[16,4,1,128]{3,2,1,0:T(1,128)S(1)} fusion(f32[16,4,128,1]{2,3,1,0:T(1,128)S(1)} %bitcast.14, f32[16,4,128,128]{3,2,1,0:T(8,128)S(1)} %multiply_add_fusion), kind=kOutput, calls=%fused_computation.30 | convolution fusion | flops 12582912 | bytes 4259840 | tf_op jit(solution)/shard_map/shd,shde->she/dot_general | solution.py:347
  18.4 0.0 copy-done.1
  18.4 0.1 fusion.7
  18.5 0.6 %copy.26 = bf16[2,8,4,128]{3,1,2,0:T(8,128)(2,1)} copy(bf16[2,8,4,128]{3,2,1,0:T(4,128)(2,1)S(1)} %bitcast.17) | data formatting | bytes 32768
  19.1 0.0 copy-done.5
  19.1 0.6 %reshape.54.gain_ref = bf16[1,1024]{1,0:T(2,128)(2,1)} reshape(bf16[1024]{0:T(1024)(128)(2,1)S(1)} %copy-done.5) | data formatting | bytes 4096 | tf_op jit(solution)/shard_map/reshape | solution.py:288
  19.7 30.8 %channel_mixer.1 = bf16[16,1024]{1,0:T(8,128)(2,1)} custom-call(bf16[16,1024]{1,0:T(8,128)(2,1)} %tokens_ref.1, bf16[16,512]{1,0:T(8,128)(2,1)} %bitcast.16, bf16[1,1024]{1,0:T(2,128)(2,1)} %reshape.54.gain_ref, bf16[1024,1024]{1,0:T(8,128)(2,1)} %out_hbm.1, bf16[1024,512]{1,0:T(8,128)(2,1)} %up_hbm.1, bf16[512,1024]{1,0:T(8,128)(2,1)} %down_hbm.1), custom_call_target="tpu_custom_call" | custom-call | tf_op jit(solution)/shard_map/channel_mixer/pallas_call | solution.py:255
  50.5 1.4 %copy.28 = bf16[16,1024]{1,0:T(8,128)(2,1)} copy(bf16[16,1024]{1,0:T(8,128)(2,1)} %channel_mixer.1) | data formatting | bytes 65536
  (7 shorter events, 0.1 us)
Async XLA Ops:
  0.6 3.2 %copy-start = (bf16[2048,512]{1,0:T(8,128)(2,1)S(1)}, bf16[2048,512]{1,0:T(8,128)(2,1)}, u32[]{:S(2)}) copy-start(bf16[2048,512]{1,0:T(8,128)(2,1)} %param.20) | copy-start | bytes 6291460
  4.2 4.1 %copy-start.3 = (bf16[2,8,2048]{2,1,0:T(8,128)(2,1)S(1)}, bf16[2,8,2048]{2,1,0:T(8,128)(2,1)}, u32[]{:S(2)}) copy-start(bf16[2,8,2048]{2,1,0:T(8,128)(2,1)} %param.21) | copy-start | bytes 196612
  4.3 4.3 %copy-start.7 = (f32[8]{0:T(128)S(1)}, f32[8]{0:T(128)}, u32[]{:S(2)}) copy-start(f32[8]{0:T(128)} %param.22) | copy-start | bytes 100
  4.3 4.4 %copy-start.6 = (f32[16,4]{0,1:T(4,128)S(1)}, f32[16,4]{0,1:T(4,128)}, u32[]{:S(2)}) copy-start(f32[16,4]{0,1:T(4,128)} %param.25) | copy-start | bytes 772
  6.3 4.6 %copy-start.2 = (f32[16,4,128]{2,1,0:T(4,128)S(1)}, f32[16,4,128]{2,1,0:T(4,128)}, u32[]{:S(2)}) copy-start(f32[16,4,128]{2,1,0:T(4,128)} %param.24) | copy-start | bytes 98308
  8.7 6.0 %copy-start.4 = (f32[16,4]{0,1:T(4,128)}, f32[16,4]{0,1:T(4,128)S(1)}, u32[]{:S(2)}) copy-start(f32[16,4]{0,1:T(4,128)S(1)} %get-tuple-element.16) | copy-start | bytes 772
  14.7 3.7 %copy-start.1 = (f32[16,4,128,128]{3,2,1,0:T(8,128)}, f32[16,4,128,128]{3,2,1,0:T(8,128)S(1)}, u32[]{:S(2)}) copy-start(f32[16,4,128,128]{3,2,1,0:T(8,128)S(1)} %multiply_add_fusion) | copy-start | bytes 12582916
  14.7 4.4 %copy-start.5 = (bf16[1024]{0:T(1024)(128)(2,1)S(1)}, bf16[1024]{0:T(1024)(128)(2,1)}, u32[]{:S(2)}) copy-start(bf16[1024]{0:T(1024)(128)(2,1)} %param.27) | copy-start | bytes 6148

commit v2 on v1

--- a/solution.py
+++ b/solution.py
@@ -29,12 +29,39 @@
     cores,
     model_width,
     tokens_ref,
-    mixed_ref,
+    attn_gain_ref,
+    gate_ref,
+    bias_ref,
+    norm_ref,
+    max_ref,
     gain_ref,
+    query_hbm,
+    key_hbm,
+    value_hbm,
+    outgate_hbm,
+    state_hbm,
     out_hbm,
     up_hbm,
     down_hbm,
     result_ref,
+    matrix_hbm,
+    next_norm_ref,
+    next_max_ref,
+    column_ref,
+    value_ref,
+    kept_ref,
+    query_w,
+    key_w,
+    value_w,
+    outgate_w,
+    state,
+    tokens_all,
+    query_t,
+    numer,
+    mixed_ref,
+    token_send_sem,
+    token_recv_sem,
+    store_sem,
     out_w,
     up_w,
     down_w,
@@ -60,7 +87,8 @@
     far_send_sem,
     far_recv_sem,
 ):
-    rows = tokens_ref.shape[0]
+    rows, features = tokens_ref.shape
+    heads, head_dim = norm_ref.shape[1:]
     width = mixed_ref.shape[1]
     hidden_width = up_w.shape[1]
     me = lax.axis_index("kv")
@@ -69,7 +97,18 @@
     spot = lax.rem(me, plane)
     loads = [
         pltpu.make_async_copy(src, dst, load_sem.at[i])
-        for i, (src, dst) in enumerate(((out_hbm, out_w), (up_hbm, up_w), (down_hbm, down_w)))
+        for i, (src, dst) in enumerate(
+            (
+                (key_hbm, key_w),
+                (query_hbm, query_w),
+                (value_hbm, value_w),
+                (outgate_hbm, outgate_w),
+                (state_hbm, state),
+                (out_hbm, out_w),
+                (up_hbm, up_w),
+                (down_hbm, down_w),
+            )
+        )
     ]
     for load in loads:
         load.start()
@@ -112,13 +151,98 @@
 
     for s in range(1, cores):
         send(
+            tokens_ref,
+            tokens_all.at[s],
+            token_send_sem.at[s],
+            token_recv_sem.at[s],
+            {"tp": core_steps[s][0]},
+        )
+    parts = []
+    squares_in = 0.0
+    for s in range(cores):
+        if s:
+            arrived(tokens_all.at[s], token_recv_sem.at[s])
+        block = (tokens_all[s] if s else tokens_ref[...]).astype(jnp.float32)
+        owned = pl.ds(pl.multiple_of(core_steps[s][1] * features, features), features)
+        squares_in = squares_in + jnp.sum(block * block, axis=1, keepdims=True)
+        block_gain = attn_gain_ref[owned].astype(jnp.float32).reshape(1, features)
+        parts.append((owned, (block * block_gain).astype(jnp.bfloat16)))
+    scale_in = lax.rsqrt(squares_in / model_width + epsilon)
+    gate_pre = sum(
+        lax.dot_general(
+            part, gate_ref[:, owned], (((1,), (1,)), ((), ())), preferred_element_type=jnp.float32
+        )
+        for owned, part in parts
+    )
+    gate_pre = gate_pre * scale_in
+    all_heads = gate_pre.shape[1] // 2
+    forget_pre = gate_pre[:, all_heads:] + bias_ref[...]
+    forget_all = jnp.minimum(forget_pre, 0.0) - jnp.log1p(jnp.exp(-jnp.abs(forget_pre)))
+    input_pre = gate_pre[:, :all_heads]
+    gate_lane = lax.broadcasted_iota(jnp.int32, input_pre.shape, 1)
+    diagonal = lax.broadcasted_iota(jnp.int32, (rows, rows), 0) == lax.broadcasted_iota(
+        jnp.int32, (rows, rows), 1
+    )
+    kept, admitted = [], []
+    for h in range(heads):
+        mine = core * heads + h
+        in_gate = jnp.sum(jnp.where(gate_lane == mine, input_pre, 0.0), axis=1, keepdims=True)
+        forget_log = jnp.sum(jnp.where(gate_lane == mine, forget_all, 0.0), axis=1, keepdims=True)
+        state_max = jnp.sum(jnp.where(diagonal, max_ref[h : h + 1, :], 0.0), axis=1, keepdims=True)
+        level = forget_log + state_max
+        next_max = jnp.maximum(level, in_gate)
+        kept.append(jnp.exp(level - next_max))
+        admitted.append(jnp.exp(in_gate - next_max))
+        next_max_ref[h : h + 1, :] = jnp.sum(
+            jnp.where(diagonal, next_max, 0.0), axis=0, keepdims=True
+        )
+        kept_ref[:, h : h + 1] = kept[h]
+
+    def project(weight, load):
+        load.wait()
+        return sum(
+            jnp.dot(part, weight[owned, :], preferred_element_type=jnp.float32)
+            for owned, part in parts
+        ) * scale_in
+
+    def head(values, h):
+        return values[:, h * head_dim : (h + 1) * head_dim]
+
+    key_rows = project(key_w, loads[0]) * head_dim ** (-0.5)
+    query_rows = project(query_w, loads[1])
+    query_t[...] = query_rows.T
+    column_ref[...] = jnp.concatenate(
+        [admitted[h] * head(key_rows, h) for h in range(heads)], axis=1
+    ).T
+    value_rows = project(value_w, loads[2])
+    value_ref[...] = value_rows
+    outgate = jax.nn.sigmoid(project(outgate_w, loads[3]))
+    loads[4].wait()
+    for h in range(heads):
+        for b in range(rows):
+            column = query_t[h * head_dim : (h + 1) * head_dim, b : b + 1]
+            numer[h, b : b + 1, :] = jnp.sum(column * state[b, h], axis=0, keepdims=True)
+    for h in range(heads):
+        query_head, key_head = head(query_rows, h), admitted[h] * head(key_rows, h)
+        next_norm = kept[h] * norm_ref[:, h, :] + key_head
+        next_norm_ref[:, h, :] = next_norm
+        denominator = jnp.sum(query_head * next_norm, axis=1, keepdims=True)
+        overlap = jnp.sum(query_head * key_head, axis=1, keepdims=True)
+        numerator = kept[h] * numer[h] + overlap * head(value_rows, h)
+        head_out = numerator / jnp.maximum(jnp.abs(denominator), 1.0)
+        mixed_ref[:, h * head_dim : (h + 1) * head_dim] = (head_out * head(outgate, h)).astype(
+            jnp.bfloat16
+        )
+
+    for s in range(1, cores):
+        send(
             mixed_ref,
             mixed_all.at[s],
             mixed_send_sem.at[s],
             mixed_recv_sem.at[s],
             {"tp": core_steps[s][0]},
         )
-    loads[0].wait()
+    loads[5].wait()
 
     def out_part(values, owner):
         block = out_w[pl.ds(pl.multiple_of(owner * width, width), width), :]
@@ -150,17 +274,33 @@
             )
 
     spread(0)
-    gain = gain_ref[...].astype(jnp.float32)
+    stores = [
+        pltpu.make_async_copy(state.at[b], matrix_hbm.at[b], store_sem.at[b]) for b in range(rows)
+    ]
+
+    def update(b):
+        for h in range(heads):
+            lanes = slice(h * head_dim, (h + 1) * head_dim)
+            share = jnp.broadcast_to(kept_ref[b : b + 1, h : h + 1], (1, head_dim))
+            state[b, h] = share * state[b, h] + column_ref[lanes, b : b + 1] * value_ref[
+                b : b + 1, lanes
+            ]
+
+    gain = gain_ref[...].astype(jnp.float32).reshape(1, features)
     group = plane * rows
 
+    def relay_stage(g):
+        arrived(rows_all.at[g, 0], row_recv_sem.at[g, 0])
+        spread(g)
+
     def up_stage(g):
-        if g + 1 < layers:
-            arrived(rows_all.at[g + 1, 0], row_recv_sem.at[g + 1, 0])
-            spread(g + 1)
+        for b in range(g * rows // layers, (g + 1) * rows // layers):
+            update(b)
+            stores[b].start()
         for s in range(1, plane):
             arrived(rows_all.at[g, s], row_recv_sem.at[g, s])
         if g == 0:
-            loads[1].wait()
+            loads[6].wait()
         values = rows_all[g].reshape(group, -1).astype(jnp.float32)
         squares = jnp.sum(values * values, axis=1, keepdims=True)
         high = squares.astype(jnp.bfloat16).astype(jnp.float32)
@@ -191,7 +331,7 @@
         up_value = total * lax.rsqrt(squares / model_width + epsilon)
         hidden = jnp.square(jnp.maximum(up_value, 0.0)).astype(jnp.bfloat16)
         if g == 0:
-            loads[2].wait()
+            loads[7].wait()
         share = jnp.dot(hidden, down_w[...], preferred_element_type=jnp.float32)
         down_own[g] = share[:rows]
         near_send[g] = share.astype(jnp.bfloat16).reshape(near_send.shape[1:])
@@ -226,10 +366,12 @@
         )
 
     for g in range(layers + 2):
+        if g + 1 < layers:
+            relay_stage(g + 1)
+        if 0 <= g - 1 < layers:
+            down_stage(g - 1)
         if g < layers:
             up_stage(g)
-        if 0 <= g - 1 < layers:
-            down_stage(g - 1)
         if 0 <= g - 2 < layers:
             far_stage(g - 2)
     total = down_own[0]
@@ -239,53 +381,33 @@
     result_ref[...] = (rows_all[0, 0].astype(jnp.float32) + total).astype(jnp.bfloat16)
     for copy in started:
         copy.wait_send()
-
-
-def channel_mixer(tokens, mixed, mlp_gain, out_weight, up_weight, down_weight, model_width):
-    count = lax.axis_size("kv")
-    cores = lax.axis_size("tp")
-    plane = 4 if count % 4 == 0 else 1
-    layers = count // plane
-    rows, features = tokens.shape
-    hidden_width = up_weight.shape[1]
-    group = plane * rows
-    bf16, f32, dma = jnp.bfloat16, jnp.float32, pltpu.SemaphoreType.DMA
-    vmem = pl.BlockSpec(memory_space=pltpu.VMEM)
-    anywhere = pl.BlockSpec(memory_space=pl.ANY)
-    return pl.pallas_call(
-        functools.partial(mixer_kernel, layers, plane, cores, model_width),
-        out_shape=jax.ShapeDtypeStruct((rows, features), bf16),
-        in_specs=[vmem] * 3 + [anywhere] * 3,
-        out_specs=vmem,
-        scratch_shapes=[
-            pltpu.VMEM(out_weight.shape, bf16),
-            pltpu.VMEM(up_weight.shape, bf16),
-            pltpu.VMEM(down_weight.shape, bf16),
-            pltpu.VMEM((cores,) + mixed.shape, bf16),
-            pltpu.VMEM((layers, plane, rows, features), bf16),
-            pltpu.VMEM((layers, group, hidden_width + 128), f32),
-            pltpu.VMEM((layers, group, hidden_width + 128), bf16),
-            pltpu.VMEM((layers, cores, group, hidden_width + 128), bf16),
-            pltpu.VMEM((layers, rows, features), f32),
-            pltpu.VMEM((layers, plane, rows, features), bf16),
-            pltpu.VMEM((layers, plane, rows, features), bf16),
-            pltpu.VMEM((layers, rows, features), bf16),
-            pltpu.VMEM((layers, rows, features), bf16),
-            dma((3,)),
-            dma((cores,)),
-            dma((cores,)),
-            dma((layers, plane)),
-            dma((layers, plane)),
-            dma((layers, cores)),
-            dma((layers, cores)),
-            dma((layers, plane)),
-            dma((layers, plane)),
-            dma((layers,)),
-            dma((layers,)),
-        ],
-        compiler_params=pltpu.CompilerParams(collective_id=0, has_side_effects=True),
-        name="channel_mixer",
-    )(tokens, mixed, mlp_gain.reshape(1, features), out_weight, up_weight, down_weight)
+    for store in stores:
+        store.wait()
+
+
+def emit_kernel(*refs):
+    sources, targets, held, (load_sem, store_sem) = refs[:4], refs[4:8], refs[8:12], refs[12:]
+    pieces = []
+    for source, target, via in zip(sources, targets, held):
+        if len(source.shape) == 4:
+            pieces += [(source.at[b], target.at[b], via.at[b]) for b in range(source.shape[0])]
+        else:
+            pieces.append((source, target, via))
+    loads = [
+        pltpu.make_async_copy(source, via, load_sem.at[i])
+        for i, (source, _, via) in enumerate(pieces)
+    ]
+    stores = [
+        pltpu.make_async_copy(via, target, store_sem.at[i])
+        for i, (_, target, via) in enumerate(pieces)
+    ]
+    for load in loads:
+        load.start()
+    for load, store in zip(loads, stores):
+        load.wait()
+        store.start()
+    for store in stores:
+        store.wait()
 
 
 def body(
@@ -305,55 +427,104 @@
     up_weight,
     down_weight,
 ):
-    sequences = tokens.shape[0]
-    local_heads = state_matrix.shape[1]
-    head_dim = state_matrix.shape[2]
+    count = lax.axis_size("kv")
+    cores = lax.axis_size("tp")
+    plane = 4 if count % 4 == 0 else 1
+    layers = count // plane
+    rows, features = tokens.shape
+    heads, head_dim = state_norm.shape[1:]
     width = query_weight.shape[1]
     model_width = attn_gain.shape[0]
-    first_head = lax.axis_index("tp") * local_heads
-    my_gates = lax.dynamic_slice_in_dim(gate_weight, first_head, local_heads, 1).reshape(
-        2 * local_heads, model_width
+    all_heads = forget_bias.shape[0]
+    hidden_width = up_weight.shape[1]
+    group = plane * rows
+    bf16, f32, dma = jnp.bfloat16, jnp.float32, pltpu.SemaphoreType.DMA
+    vmem = pl.BlockSpec(memory_space=pltpu.VMEM)
+    anywhere = pl.BlockSpec(memory_space=pl.ANY)
+    shape = jax.ShapeDtypeStruct
+    outputs = pl.pallas_call(
+        functools.partial(mixer_kernel, layers, plane, cores, model_width),
+        out_shape=(
+            shape((rows, features), bf16),
+            shape(state_matrix.shape, f32),
+            shape(state_norm.shape, f32),
+            shape((heads, rows), f32),
+        ),
+        in_specs=[vmem] * 7 + [anywhere] * 8,
+        out_specs=(vmem, anywhere, vmem, vmem),
+        scratch_shapes=[
+            pltpu.VMEM((width, rows), f32),
+            pltpu.VMEM((rows, width), f32),
+            pltpu.VMEM((rows, heads), f32),
+            pltpu.VMEM(query_weight.shape, bf16),
+            pltpu.VMEM(key_weight.shape, bf16),
+            pltpu.VMEM(value_weight.shape, bf16),
+            pltpu.VMEM(outgate_weight.shape, bf16),
+            pltpu.VMEM(state_matrix.shape, f32),
+            pltpu.VMEM((cores,) + tokens.shape, bf16),
+            pltpu.VMEM((width, rows), f32),
+            pltpu.VMEM((heads, rows, head_dim), f32),
+            pltpu.VMEM((rows, width), bf16),
+            dma((cores,)),
+            dma((cores,)),
+            dma((rows,)),
+            pltpu.VMEM(out_weight.shape, bf16),
+            pltpu.VMEM(up_weight.shape, bf16),
+            pltpu.VMEM(down_weight.shape, bf16),
+            pltpu.VMEM((cores, rows, width), bf16),
+            pltpu.VMEM((layers, plane, rows, features), bf16),
+            pltpu.VMEM((layers, group, hidden_width + 128), f32),
+            pltpu.VMEM((layers, group, hidden_width + 128), bf16),
+            pltpu.VMEM((layers, cores, group, hidden_width + 128), bf16),
+            pltpu.VMEM((layers, rows, features), f32),
+            pltpu.VMEM((layers, plane, rows, features), bf16),
+            pltpu.VMEM((layers, plane, rows, features), bf16),
+            pltpu.VMEM((layers, rows, features), bf16),
+            pltpu.VMEM((layers, rows, features), bf16),
+            dma((8,)),
+            dma((cores,)),
+            dma((cores,)),
+            dma((layers, plane)),
+            dma((layers, plane)),
+            dma((layers, cores)),
+            dma((layers, cores)),
+            dma((layers, plane)),
+            dma((layers, plane)),
+            dma((layers,)),
+            dma((layers,)),
+        ],
+        compiler_params=pltpu.CompilerParams(
+            collective_id=0, has_side_effects=True, vmem_limit_bytes=58000 * 1024
+        ),
+        name="layer",
+    )(
+        tokens,
+        attn_gain,
+        gate_weight.reshape(2 * all_heads, model_width),
+        forget_bias.reshape(1, all_heads),
+        state_norm,
+        state_max.T,
+        mlp_gain,
+        query_weight,
+        key_weight,
+        value_weight,
+        outgate_weight,
+        state_matrix,
+        out_weight,
+        up_weight,
+        down_weight,
     )
-    my_bias = lax.dynamic_slice_in_dim(forget_bias, first_head, local_heads, 0)
-    gain_full = attn_gain.astype(jnp.float32)
-    seg_values = lax.all_gather(tokens, "tp", axis=1, tiled=True).astype(jnp.float32)
-    scaled = (seg_values * gain_full).astype(jnp.bfloat16)
-
-    def product(weight):
-        return jnp.dot(scaled, weight, preferred_element_type=jnp.float32)
-
-    gate_part = jnp.einsum("sd,gd->sg", scaled, my_gates, preferred_element_type=jnp.float32)
-    squares = jnp.sum(seg_values * seg_values, axis=1)
-    query_acc = product(query_weight)
-    key_acc = product(key_weight)
-    value_acc = product(value_weight)
-    outgate_acc = product(outgate_weight)
-    scale_in = lax.rsqrt(squares / model_width + epsilon)[:, None]
-    query_rows = (query_acc * scale_in).reshape(sequences, local_heads, head_dim)
-    key_rows = (key_acc * scale_in * head_dim ** (-0.5)).reshape(sequences, local_heads, head_dim)
-    value_rows = (value_acc * scale_in).reshape(sequences, local_heads, head_dim)
-    outgate = (outgate_acc * scale_in).reshape(sequences, local_heads, head_dim)
-    gate_pre = gate_part * scale_in
-    in_gate = gate_pre[:, :local_heads]
-    forget_log = jax.nn.log_sigmoid(gate_pre[:, local_heads:] + my_bias)
-    next_max = jnp.maximum(forget_log + state_max, in_gate)
-    kept_share = jnp.exp(forget_log + state_max - next_max)
-    admitted = jnp.exp(in_gate - next_max)
-    next_matrix = (
-        kept_share[:, :, None, None] * state_matrix
-        + admitted[:, :, None, None] * key_rows[:, :, :, None] * value_rows[:, :, None, :]
-    )
-    next_norm = kept_share[:, :, None] * state_norm + admitted[:, :, None] * key_rows
-    numerator = jnp.einsum(
-        "shd,shde->she", query_rows, next_matrix, precision=lax.Precision.HIGHEST
-    )
-    denominator = jnp.sum(query_rows * next_norm, axis=2)
-    head_out = numerator / jnp.maximum(jnp.abs(denominator), 1.0)[:, :, None]
-    mixed = (head_out * jax.nn.sigmoid(outgate)).reshape(sequences, width).astype(jnp.bfloat16)
-    result = channel_mixer(
-        tokens, mixed, mlp_gain, out_weight, up_weight, down_weight, model_width
-    )
-    return (result, next_matrix, next_norm, next_max)
+    result, next_matrix, next_norm, next_max = pl.pallas_call(
+        emit_kernel,
+        out_shape=tuple(shape(x.shape, x.dtype) for x in outputs),
+        in_specs=[anywhere] * 4,
+        out_specs=(anywhere,) * 4,
+        scratch_shapes=[pltpu.VMEM(x.shape, x.dtype) for x in outputs]
+        + [dma((rows + 3,)), dma((rows + 3,))],
+        compiler_params=pltpu.CompilerParams(vmem_limit_bytes=58000 * 1024),
+        name="emit",
+    )(*outputs)
+    return (result, next_matrix, next_norm, next_max.T)
 
 
 def solution(mesh):

time: 52.3 us -> 39.7 us (0.76)
  matrix products: 10 us -> 0 us
  Pallas kernels: 30.8 us -> 38.9 us
  other arithmetic: 4.78 us -> 0 us
  local copies, waits for them, and re-layouts: 3.14 us -> 0 us
  blocking collectives: 2.34 us -> 0 us
    dot_general x6 -> x0, matrix products: 10 us -> none  [the longest x4 6.22 us: product(): return jnp.dot(scaled, weight, preferred_element_type=jnp.float32)]
    pallas_call x1 -> x2, Pallas kernels: 30.8 us -> 38.9 us  [the longest x1 34.9 us: body(): pl.pallas_call(functools.partial(mixer_kernel, layers, plane, cores, mode...]
    add x1 -> x0, other arithmetic: 3.04 us -> none  [body(): kept_share[:, :, None, None] * state_matrix]
    all_gather x1 -> x0, blocking collectives: 2.34 us -> none  [body(): lax.all_gather(tokens, 'tp', axis=1, tiled=True).astype(jnp.float32)]
    unnamed x18 -> x0, local copies, waits for them, and re-layouts: 2.04 us -> none
    reduce_sum x2 -> x0, other arithmetic: 0.85 us -> none  [the longest x1 0.72 us: body(): denominator = jnp.sum(query_rows * next_norm, axis=2)]
    convert_element_type x2 -> x0, other arithmetic: 0.79 us -> none  [the longest x1 0.69 us: body(): gain_full = attn_gain.astype(jnp.float32)]
    reshape x4 -> x0, local copies, waits for them, and re-layouts: 0.69 us -> none  [the longest x1 0.6 us: channel_mixer(): mlp_gain.reshape(1, features)]
where the time goes in v2:
time: 39.7 us; the launch traced here: 39.5 us
  Pallas kernels  38.9 us (98%)
  between operations  0.65 us (2%)
    pallas_call x1, Pallas kernels, body(): pl.pallas_call(functools.partial(mixer_kernel, layers, plane, cores, mode...  34.9 us
    pallas_call x1, Pallas kernels, body(): pl.pallas_call(emit_kernel, out_shape=tuple((shape(x.shape, x.dtype) for...  3.96 us

profile of v2, /device:TPU:0, one launch (start us, length us, event | category | flops | bytes accessed | tf_op | source)
XLA Modules:
  0.0 39.5 jit_solution(4454858132524071696)
XLA Ops:
  0.6 34.9 %layer.1 = (bf16[16,1024]{1,0:T(8,128)(2,1)}, f32[16,4,128,128]{3,2,1,0:T(8,128)}, f32[16,4,128]{2,1,0:T(4,128)}, f32[4,16]{1,0:T(4,128)}) custom-call(bf16[16,1024]{1,0:T(8,128)(2,1)} %tokens_ref.1, bf16[2048]{0:T(1024)(128)(2,1)} %attn_gain_ref.1, bf16[16,2048]{1,0:T(8,128)(2,1)} %bitcast.4, f32[1,8]{1,0:T(1,128)} %bitcast.6, f32[16,4,128]{2,1,0:T(4,128)} %norm_ref.1, ...), custom_call_target="tpu_custom_call" | custom-call | tf_op jit(solution)/shard_map/layer/pallas_call | solution.py:445
  35.6 4.0 %emit.1 = (bf16[16,1024]{1,0:T(8,128)(2,1)}, f32[16,4,128,128]{3,2,1,0:T(8,128)}, f32[16,4,128]{2,1,0:T(4,128)}, f32[4,16]{1,0:T(4,128)}) custom-call(bf16[16,1024]{1,0:T(8,128)(2,1)} %get-tuple-element.12.refs_0_, f32[16,4,128,128]{3,2,1,0:T(8,128)} %get-tuple-element.13.refs_1_, f32[16,4,128]{2,1,0:T(4,128)} %get-tuple-element.14.refs_2_, ...), custom_call_target="tpu_custom_call" | custom-call | tf_op jit(solution)/shard_map/emit/pallas_call | solution.py:517
